TPU v7x, 32 devices: a whole 2x2x4 slice. The times are simulated.
32 devices in a mesh: sp: 8 (over z, x), tp: 4 (over y, core).
Axes of the slice: x: 2, y: 2, z: 4, core: 2. Of those that a mesh axis runs over, the one named last changes fastest.
Arguments:
- residual: bfloat16 [2048, 2048], P('sp', 'tp'), may hold values from -8 to 8
- query_latent: bfloat16 [2048, 512], P('sp'), may hold values from -6 to 6
- shared_latent: bfloat16 [2048, 256], P('sp'), may hold values from -6 to 6
- rotary_key: bfloat16 [2048, 32], P('sp'), may hold values from -300 to 300
- query_gain: float32 [512], replicated, may hold values from 0.1 to 1.9
- latent_gain: float32 [256], replicated, may hold values from 0.1 to 1.9
- query_narrow: bfloat16 [512, 384], P(None, 'tp'), may hold values from -0.5 to 0.5
- key_narrow: bfloat16 [256, 256], P(None, 'tp'), may hold values from -0.375 to 0.375
- value_narrow: bfloat16 [256, 256], P(None, 'tp'), may hold values from -0.375 to 0.375
- query_wide: bfloat16 [512, 640], P(None, 'tp'), may hold values from -0.5 to 0.5
- key_wide: bfloat16 [256, 512], P(None, 'tp'), may hold values from -0.375 to 0.375
- value_wide: bfloat16 [256, 512], P(None, 'tp'), may hold values from -0.375 to 0.375
- output_narrow: bfloat16 [256, 2048], P('tp'), may hold values from -1.75 to 1.75
- output_wide: bfloat16 [512, 2048], P('tp'), may hold values from -1.75 to 1.75
- first_gain: float32 [2048], P('tp'), may hold values from 0.1 to 1.9
- first_bias: float32 [2048], P('tp'), may hold values from -1.5 to 1.5
- gate_weight: bfloat16 [2048, 5632], P('sp', 'tp'), may hold values from -0.125 to 0.125
- up_weight: bfloat16 [2048, 5632], P('sp', 'tp'), may hold values from -0.125 to 0.125
- down_weight: bfloat16 [5632, 2048], P('tp', 'sp'), may hold values from -0.078125 to 0.078125
- second_gain: float32 [2048], P('tp'), may hold values from 0.1 to 1.9
- second_bias: float32 [2048], P('tp'), may hold values from -1.5 to 1.5
Outputs:
- layer_out: bfloat16 [2048, 2048], P('sp', 'tp')
All inputs are finite; a program needn't handle non-finite values.
Results may differ from a plain program's by a relative error of at most 0.017.
The roundings to bfloat16 on the way count: a program that leaves them out, or rounds other values in their place, can miss the bound.
Values may be sent and summed in bfloat16 or wider, within the bound.
No kernel may reach another device: no remote copies, remote signals or barrier semaphores. Data moves between devices by JAX's collectives and lax.ppermute only.
A program may use at most 192 MiB of HBM per device.

v0:
```python
import jax
import jax.numpy as jnp
from jax import lax
from jax.sharding import PartitionSpec as P

ROPE = 32
NOPE_A = 64
V_A = 64
NOPE_B = 128
V_B = 128
GRID_W = 64
EPS_ROOT = 1e-06
EPS_LAYER = 1e-05
THETA = 10000.0
DEEP_ALPHA = 2.0**0.25


def rotate(half_part, angle):
    lower, upper = jnp.split(half_part, 2, axis=-1)
    cosine = jnp.cos(angle)
    sine = jnp.sin(angle)
    return jnp.concatenate([lower * cosine - upper * sine, upper * cosine + lower * sine], axis=-1)


def turn_axial(values_in, positions):
    quarter = values_in.shape[-1] // 4
    freqs = THETA ** (-(2.0 * jnp.arange(quarter, dtype=jnp.float32)) / (2 * quarter))
    row_angle = (positions // GRID_W).astype(jnp.float32)[:, None, None] * freqs
    col_angle = (positions % GRID_W).astype(jnp.float32)[:, None, None] * freqs
    first_half, second_half = jnp.split(values_in, 2, axis=-1)
    return jnp.concatenate([rotate(first_half, row_angle), rotate(second_half, col_angle)], axis=-1)


def root_scale(latent, gain):
    floated = latent.astype(jnp.float32)
    return (
        floated * lax.rsqrt(jnp.mean(floated * floated, axis=-1, keepdims=True) + EPS_ROOT) * gain
    )


def make_query(normed, weight, plain_dim, positions):
    product = jnp.dot(normed, weight, preferred_element_type=jnp.float32)
    head_count = weight.shape[1] // (plain_dim + ROPE)
    product = product.reshape(product.shape[0], head_count, plain_dim + ROPE)
    turned = turn_axial(product[:, :, plain_dim:], positions)
    return jnp.concatenate([product[:, :, :plain_dim], turned], axis=-1).astype(jnp.bfloat16)


def fresh_state(row_count, head_count, value_dim):
    largest = jnp.full((head_count, row_count), -jnp.inf, jnp.float32)
    totals = jnp.zeros((head_count, row_count), jnp.float32)
    weighted = jnp.zeros((row_count, head_count, value_dim), jnp.float32)
    return (largest, totals, weighted)


def update(state_now, queries, key_rows, value_rows, rotary_rows, plain_dim):
    largest, totals, weighted = state_now
    score_scale = queries.shape[2] ** (-0.5)
    scores = jnp.einsum(
        "qhd,khd->hqk", queries[:, :, :plain_dim], key_rows, preferred_element_type=jnp.float32
    )
    scores = scores + jnp.einsum(
        "qhd,kd->hqk", queries[:, :, plain_dim:], rotary_rows, preferred_element_type=jnp.float32
    )
    scores = scores * score_scale
    new_largest = jnp.max(scores, axis=-1)
    factor = jnp.exp(largest - new_largest)
    raised = jnp.exp(scores - new_largest[:, :, None])
    totals = totals * factor + jnp.sum(raised, axis=-1)
    added = jnp.einsum(
        "hqk,khd->qhd", raised.astype(jnp.bfloat16), value_rows, preferred_element_type=jnp.float32
    )
    weighted = weighted * factor.T[:, :, None] + added
    return (new_largest, totals, weighted)


def finish(state_now):
    largest, totals, weighted = state_now
    output = (weighted / totals.T[:, :, None]).astype(jnp.bfloat16)
    return output.reshape(output.shape[0], output.shape[1] * output.shape[2])


def finish_norm(summed, sums, squares, gain, bias, width_total):
    center = sums / width_total
    spread = squares / width_total - center * center
    normed = (summed - center[:, None]) * lax.rsqrt(spread + EPS_LAYER)[:, None]
    return (normed * gain + bias).astype(jnp.bfloat16)


def body(
    residual,
    query_latent,
    shared_latent,
    rotary_key,
    query_gain,
    latent_gain,
    query_narrow,
    key_narrow,
    value_narrow,
    query_wide,
    key_wide,
    value_wide,
    output_narrow,
    output_wide,
    first_gain,
    first_bias,
    gate_weight,
    up_weight,
    down_weight,
    second_gain,
    second_bias,
):
    row_count = residual.shape[0]
    offset = lax.axis_index("sp") * row_count
    positions = offset + jnp.arange(row_count, dtype=jnp.int32)
    query_normed = root_scale(query_latent, query_gain).astype(jnp.bfloat16)
    narrow_queries = make_query(query_normed, query_narrow, NOPE_A, positions)
    wide_queries = make_query(query_normed, query_wide, NOPE_B, positions)
    narrow_heads = narrow_queries.shape[1]
    wide_heads = wide_queries.shape[1]
    start_state = (
        fresh_state(row_count, narrow_heads, V_A),
        fresh_state(row_count, wide_heads, V_B),
    )
    shard_rows = (
        lax.all_gather(shared_latent, "sp", axis=0, tiled=True),
        lax.all_gather(rotary_key, "sp", axis=0, tiled=True),
    )
    latent_rows = shard_rows[0]
    normed = root_scale(latent_rows, latent_gain).astype(jnp.bfloat16)
    count = latent_rows.shape[0]
    narrow_keys = jnp.dot(normed, key_narrow, preferred_element_type=jnp.float32).astype(
        jnp.bfloat16
    )
    narrow_vals = jnp.dot(normed, value_narrow, preferred_element_type=jnp.float32).astype(
        jnp.bfloat16
    )
    wide_keys = jnp.dot(normed, key_wide, preferred_element_type=jnp.float32).astype(jnp.bfloat16)
    wide_vals = jnp.dot(normed, value_wide, preferred_element_type=jnp.float32).astype(jnp.bfloat16)
    key_positions = jnp.arange(count, dtype=jnp.int32)
    rotated = turn_axial(shard_rows[1].astype(jnp.float32)[:, None, :], key_positions)[
        :, 0, :
    ].astype(jnp.bfloat16)
    count = rotated.shape[0]
    narrow_state = update(
        start_state[0],
        narrow_queries,
        narrow_keys.reshape(count, narrow_heads, NOPE_A),
        narrow_vals.reshape(count, narrow_heads, V_A),
        rotated,
        NOPE_A,
    )
    wide_state = update(
        start_state[1],
        wide_queries,
        wide_keys.reshape(count, wide_heads, NOPE_B),
        wide_vals.reshape(count, wide_heads, V_B),
        rotated,
        NOPE_B,
    )
    narrow_out = finish(narrow_state)
    wide_out = finish(wide_state)
    terms = jnp.dot(narrow_out, output_narrow, preferred_element_type=jnp.float32)
    terms = terms + jnp.dot(wide_out, output_wide, preferred_element_type=jnp.float32)
    mixed = lax.psum_scatter(
        terms.astype(jnp.bfloat16), "tp", scatter_dimension=1, tiled=True
    ).astype(jnp.float32)
    width_total = mixed.shape[1] * lax.axis_size("tp")
    summed = DEEP_ALPHA * residual.astype(jnp.float32) + mixed
    sums, squares = lax.psum((jnp.sum(summed, axis=1), jnp.sum(summed * summed, axis=1)), "tp")
    normed_first = finish_norm(summed, sums, squares, first_gain, first_bias, width_total)
    full_rows = lax.all_gather(normed_first, "tp", axis=1, tiled=True)
    shard_rows = (
        lax.all_gather(gate_weight, "sp", axis=0, tiled=True),
        lax.all_gather(up_weight, "sp", axis=0, tiled=True),
    )
    gate_part = jnp.dot(full_rows, shard_rows[0], preferred_element_type=jnp.float32)
    lifted_part = jnp.dot(full_rows, shard_rows[1], preferred_element_type=jnp.float32)
    hidden = (jax.nn.silu(gate_part) * lifted_part).astype(jnp.bfloat16)
    feed_terms = jnp.dot(
        hidden,
        lax.all_gather(down_weight, "sp", axis=1, tiled=True),
        preferred_element_type=jnp.float32,
    )
    feed = lax.psum_scatter(
        feed_terms.astype(jnp.bfloat16), "tp", scatter_dimension=1, tiled=True
    ).astype(jnp.float32)
    summed_two = DEEP_ALPHA * normed_first.astype(jnp.float32) + feed
    sums_two, squares_two = lax.psum(
        (jnp.sum(summed_two, axis=1), jnp.sum(summed_two * summed_two, axis=1)), "tp"
    )
    return finish_norm(summed_two, sums_two, squares_two, second_gain, second_bias, width_total)


def solution(mesh):
    return jax.shard_map(
        body,
        mesh=mesh,
        in_specs=(
            P("sp", "tp"),
            P("sp", None),
            P("sp", None),
            P("sp", None),
            P(),
            P(),
            P(None, "tp"),
            P(None, "tp"),
            P(None, "tp"),
            P(None, "tp"),
            P(None, "tp"),
            P(None, "tp"),
            P("tp", None),
            P("tp", None),
            P("tp"),
            P("tp"),
            P("sp", "tp"),
            P("sp", "tp"),
            P("tp", "sp"),
            P("tp"),
            P("tp"),
        ),
        out_specs=P("sp", "tp"),
        check_vma=False,
    )
```

profile of v0, /device:TPU:0, one launch (start us, length us, event | category | flops | bytes accessed | tf_op | source)
XLA Modules:
  0.0 453.0 jit_solution(9527016040940097273)
XLA Ops:
  6.5 0.7 all-gather.6.cloned.1.call-update
  7.3 0.0 reduce-scatter.3.cloned.1.call-start
  7.4 32.8 %all_gather.19 = bf16[2048,32]{0,1:T(8,128)(2,1)S(1)} all-gather(bf16[256,32]{0,1:T(8,128)(2,1)} %param.24), channel_id=1, replica_groups=mesh['sp'=8,'tp'=4] {'sp'}, dimensions={0}, use_global_device_ids=true | all-gather | bytes 147456 | tf_op jit(solution)/shard_map/all_gather | solution.py:127
  40.2 1.1 fusion.31
  41.3 1.3 convolution_bitcast_fusion.5
  42.6 1.3 convolution_bitcast_fusion.4
  43.9 0.2 fusion.97
  44.1 0.6 fusion.59
  44.7 7.9 %all-gather.6.cloned.1.call-done = bf16[2048,256]{1,0:T(8,128)(2,1)} async-done(((bf16[256,256]{1,0:T(8,128)(2,1)}), bf16[2048,256]{1,0:T(8,128)(2,1)}) %all-gather.6.cloned.1.call-update) | async-done | bytes 1048592 | tf_op jit(solution)/shard_map/all_gather | solution.py:126
  52.5 1.6 fusion.6
  54.1 2.1 convolution_bitcast_fusion.3
  56.3 0.6 fusion.132
  56.9 1.3 copy-done.2
  58.2 0.4 fusion.9
  58.6 0.2 copy-done.1
  58.8 2.2 convolution_bitcast_fusion.1
  61.1 2.1 fusion.131
  63.2 1.3 copy-done.3
  64.6 0.4 fusion.11
  65.0 2.6 fusion.20
  67.6 1.8 fusion.133
  69.4 2.6 fusion.24
  72.1 3.1 fusion.4
  75.2 0.0 reduce-scatter.3.cloned.1.call-update
  75.2 0.0 all-gather.8.cloned.1.call-start
  75.2 23.7 %reduce-scatter.3.cloned.1.call-done = bf16[256,512]{1,0:T(8,128)(2,1)} async-done(((bf16[256,2048]{1,0:T(8,128)(2,1)}), bf16[256,512]{1,0:T(8,128)(2,1)}) %reduce-scatter.3.cloned.1.call-update) | async-done | bytes 262160 | tf_op jit(solution)/shard_map/reduce_scatter | solution.py:165
  99.0 1.2 fusion.34
  100.1 5.8 %all-reduce.1 = (f32[256]{0:T(256)S(1)}, f32[256]{0:T(256)S(1)}) all-reduce(f32[256]{0:T(256)S(1)} %get-tuple-element.8, f32[256]{0:T(256)S(1)} %get-tuple-element.7), channel_id=1, replica_groups=mesh['sp'=8,'tp'=4] {'tp'}, use_global_device_ids=true, to_apply=%region_10.11 | all-reduce | flops 512 | bytes 4096 | tf_op jit(solution)/shard_map/psum | solution.py:170
  105.9 1.8 add_convert_fusion.1
  107.7 0.0 all-gather.8.cloned.1.call-update
  107.7 0.0 all-gather.10.cloned.1.call-start
  107.8 0.5 all-gather.10.cloned.1.call-update
  108.3 0.0 all-gather.12.cloned.1.call-start
  108.4 0.5 all-gather.12.cloned.1.call-update
  108.9 0.0 all-gather.14.cloned.1.call-start
  109.0 0.5 all-gather.14.cloned.1.call-update
  109.5 0.2 reduce-scatter.5.cloned.1.call-start
  109.7 15.5 %all-gather.8.cloned.1.call-done = bf16[256,2048]{1,0:T(8,128)(2,1)} async-done(((bf16[256,512]{1,0:T(8,128)(2,1)}), bf16[256,2048]{1,0:T(8,128)(2,1)}) %all-gather.8.cloned.1.call-update) | async-done | bytes 1048592 | tf_op jit(solution)/shard_map/all_gather | solution.py:172
  125.2 94.4 %all-gather.10.cloned.1.call-done = bf16[2048,1408]{1,0:T(8,128)(2,1)} async-done(((bf16[256,1408]{1,0:T(8,128)(2,1)}), bf16[2048,1408]{1,0:T(8,128)(2,1)}) %all-gather.10.cloned.1.call-update) | async-done | bytes 5767184 | tf_op jit(solution)/shard_map/all_gather | solution.py:174
  219.6 4.8 %fusion.134 = f32[256,1408]{1,0:T(8,128)S(1)} fusion(bf16[256,2048]{1,0:T(8,128)(2,1)} %all-gather.8.cloned.1.call-done, bf16[2048,1408]{1,0:T(8,128)(2,1)} %all-gather.10.cloned.1.call-done), kind=kOutput, calls=%fused_computation.179 | convolution fusion | flops 1476395008 | bytes 8257536 | tf_op jit(solution)/shard_map/dot_general | solution.py:177
  224.4 87.8 %all-gather.12.cloned.1.call-done = bf16[2048,1408]{1,0:T(8,128)(2,1)} async-done(((bf16[256,1408]{1,0:T(8,128)(2,1)}), bf16[2048,1408]{1,0:T(8,128)(2,1)}) %all-gather.12.cloned.1.call-update) | async-done | bytes 5767184 | tf_op jit(solution)/shard_map/all_gather | solution.py:175
  312.2 93.2 %all-gather.14.cloned.1.call-done = bf16[1408,2048]{1,0:T(8,128)(2,1)} async-done(((bf16[1408,256]{1,0:T(8,128)(2,1)}), bf16[1408,2048]{1,0:T(8,128)(2,1)}) %all-gather.14.cloned.1.call-update) | async-done | bytes 5767184 | tf_op jit(solution)/shard_map/all_gather | solution.py:182
  405.4 8.8 %convolution_convert_fusion = bf16[256,2048]{1,0:T(8,128)(2,1)} fusion(bf16[1408,2048]{1,0:T(8,128)(2,1)} %all-gather.14.cloned.1.call-done, bf16[256,2048]{1,0:T(8,128)(2,1)S(1)} %copy-done.14, bf16[2048,1408]{1,0:T(8,128)(2,1)} %all-gather.12.cloned.1.call-done, f32[256,1408]{1,0:T(8,128)S(1)} %fusion.134), kind=kOutput, calls=%fused_computation.14 | convolution fusion | flops 2955476992 | bytes 15073280 | tf_op jit(solution)/shard_map/dot_general | solution.py:180
  414.2 0.0 reduce-scatter.5.cloned.1.call-update
  414.2 23.1 %reduce-scatter.5.cloned.1.call-done = bf16[256,512]{1,0:T(8,128)(2,1)} async-done(((bf16[256,2048]{1,0:T(8,128)(2,1)}), bf16[256,512]{1,0:T(8,128)(2,1)}) %reduce-scatter.5.cloned.1.call-update) | async-done | bytes 262160 | tf_op jit(solution)/shard_map/reduce_scatter | solution.py:185
  437.4 1.2 fusion.35
  438.5 5.8 %all-reduce = (f32[256]{0:T(256)S(1)}, f32[256]{0:T(256)S(1)}) all-reduce(f32[256]{0:T(256)S(1)} %get-tuple-element.6, f32[256]{0:T(256)S(1)} %get-tuple-element.5), channel_id=1, replica_groups=mesh['sp'=8,'tp'=4] {'tp'}, use_global_device_ids=true, to_apply=%region_15.16 | all-reduce | flops 512 | bytes 4096 | tf_op jit(solution)/shard_map/psum | solution.py:189
  444.3 1.8 add_convert_fusion
  (42 shorter events, 0.2 us)
Async XLA Ops:
  6.5 61.1 %copy-start = (bf16[128,2048]{1,0:T(8,128)(2,1)S(1)}, bf16[128,2048]{1,0:T(8,128)(2,1)}, u32[]{:S(2)}) copy-start(bf16[128,2048]{1,0:T(8,128)(2,1)} %param.34) | copy-start | bytes 1572868
  6.5 47.6 %copy-start.9 = (f32[256]{0:T(256)S(1)}, f32[256]{0:T(256)}, u32[]{:S(2)}) copy-start(f32[256]{0:T(256)} %param.26) | copy-start | bytes 3076
  6.5 47.6 %copy-start.8 = (bf16[256,64]{0,1:T(8,128)(2,1)S(1)}, bf16[256,64]{0,1:T(8,128)(2,1)}, u32[]{:S(2)}) copy-start(bf16[256,64]{0,1:T(8,128)(2,1)} %param.28) | copy-start | bytes 98308
  6.5 46.0 %all-gather.6.cloned.1.call-start = ((), (), s32[]{:S(2)}) async-start(), calls=%async_computation.2 | async-start | bytes 1179648 | tf_op jit(solution)/shard_map/all_gather | solution.py:126
  7.3 91.7 %reduce-scatter.3.cloned.1.call-start = ((), (), s32[]{:S(2)}) async-start(), calls=%async_computation.3 | async-start | bytes 1310720 | tf_op jit(solution)/shard_map/reduce_scatter | solution.py:165
  56.8 1.3 copy-start.2
  56.9 2.0 copy-start.1
  56.9 2.0 copy-start.7
  63.2 1.3 copy-start.3
  63.2 1.8 copy-start.15
  67.6 1.8 copy-start.16
  69.4 2.6 copy-start.6
  72.1 26.9 %copy-start.5 = (bf16[256,512]{1,0:T(8,128)(2,1)S(1)}, bf16[256,512]{1,0:T(8,128)(2,1)}, u32[]{:S(2)}) copy-start(bf16[256,512]{1,0:T(8,128)(2,1)} %param.21) | copy-start | bytes 786436
  72.1 33.8 %copy-start.10 = (f32[512]{0:T(512)S(1)}, f32[512]{0:T(512)}, u32[]{:S(2)}) copy-start(f32[512]{0:T(512)} %param.36) | copy-start | bytes 6148
  72.1 33.8 %copy-start.11 = (f32[512]{0:T(512)S(1)}, f32[512]{0:T(512)}, u32[]{:S(2)}) copy-start(f32[512]{0:T(512)} %param.35) | copy-start | bytes 6148
  75.2 50.0 %all-gather.8.cloned.1.call-start = ((), (), s32[]{:S(2)}) async-start(), calls=%async_computation.4 | async-start | bytes 1310720 | tf_op jit(solution)/shard_map/all_gather | solution.py:172
  107.7 111.8 %all-gather.10.cloned.1.call-start = ((), (), s32[]{:S(2)}) async-start(), calls=%async_computation.5 | async-start | bytes 6488064 | tf_op jit(solution)/shard_map/all_gather | solution.py:174
  108.3 203.8 %all-gather.12.cloned.1.call-start = ((), (), s32[]{:S(2)}) async-start(), calls=%async_computation.6 | async-start | bytes 6488064 | tf_op jit(solution)/shard_map/all_gather | solution.py:175
  108.9 296.5 %all-gather.14.cloned.1.call-start = ((), (), s32[]{:S(2)}) async-start(), calls=%async_computation.7 | async-start | bytes 6488064 | tf_op jit(solution)/shard_map/all_gather | solution.py:182
  109.5 327.9 %reduce-scatter.5.cloned.1.call-start = ((), (), s32[]{:S(2)}) async-start(), calls=%async_computation.8 | async-start | bytes 1310720 | tf_op jit(solution)/shard_map/reduce_scatter | solution.py:185
  125.2 280.2 %copy-start.14 = (bf16[256,2048]{1,0:T(8,128)(2,1)S(1)}, bf16[256,2048]{1,0:T(8,128)(2,1)}, u32[]{:S(2)}) copy-start(bf16[256,2048]{1,0:T(8,128)(2,1)} %all-gather.8.cloned.1.call-done) | copy-start | bytes 3145732
  224.4 213.0 %copy-start.4 = (bf16[256,512]{1,0:T(8,128)(2,1)S(1)}, bf16[256,512]{1,0:T(8,128)(2,1)}, u32[]{:S(2)}) copy-start(bf16[256,512]{1,0:T(8,128)(2,1)} %add_convert_fusion.1) | copy-start | bytes 786436
  224.4 219.9 %copy-start.12 = (f32[512]{0:T(512)S(1)}, f32[512]{0:T(512)}, u32[]{:S(2)}) copy-start(f32[512]{0:T(512)} %param.41) | copy-start | bytes 6148
  224.4 219.9 %copy-start.13 = (f32[512]{0:T(512)S(1)}, f32[512]{0:T(512)}, u32[]{:S(2)}) copy-start(f32[512]{0:T(512)} %param.40) | copy-start | bytes 6148
Sparse Core Ops, SparseCore 0:
  9.5 43.0 all-gather.5
  75.3 23.6 reduce-scatter.2
  107.9 17.3 all-gather.7
  127.3 92.2 all-gather.9
  221.6 90.4 all-gather.11
  314.0 91.2 all-gather.13
  414.4 22.9 reduce-scatter.4
where the time goes:
time: 454 us; the launch traced here: 453 us
  waiting for transfers between devices  348 us (77%)
  blocking collectives  44.4 us (10%)
  matrix products  33.3 us (7%)
  between operations  13.7 us (3%)
  other arithmetic  10.3 us (2%)
    all_gather x1, waiting for transfers between devices, body(): lax.all_gather(gate_weight, 'sp', axis=0, tiled=True)  94.4 us
    all_gather x1, waiting for transfers between devices, body(): lax.all_gather(down_weight, 'sp', axis=1, tiled=True)  93.2 us
    all_gather x1, waiting for transfers between devices, body(): lax.all_gather(up_weight, 'sp', axis=0, tiled=True)  87.8 us
    all_gather x1, blocking collectives, body(): lax.all_gather(rotary_key, 'sp', axis=0, tiled=True)  32.8 us
    reduce_scatter x1, waiting for transfers between devices, body(): lax.psum_scatter(terms.astype(jnp.bfloat16), 'tp', scatter_dimension=1, t...  23.7 us
    reduce_scatter x1, waiting for transfers between devices, body(): lax.psum_scatter(feed_terms.astype(jnp.bfloat16), 'tp', scatter_dimension...  23.1 us
    all_gather x1, waiting for transfers between devices, body(): full_rows = lax.all_gather(normed_first, 'tp', axis=1, tiled=True)  15.5 us
  transfers between devices with their start and end apart: 7, of which 7 were waited for; matrix products, arithmetic and copies ran while one was open for 2% of the time, Pallas kernels for 0%

commit v1 on v0

--- a/solution.py
+++ b/solution.py
@@ -13,6 +13,11 @@
 EPS_LAYER = 1e-05
 THETA = 10000.0
 DEEP_ALPHA = 2.0**0.25
+
+
+def stack_and_merge(x, axis, d):
+    blocks = lax.all_gather(x, axis)
+    return jnp.concatenate(blocks, axis=d)
 
 
 def rotate(half_part, angle):
@@ -178,9 +183,7 @@
     lifted_part = jnp.dot(full_rows, shard_rows[1], preferred_element_type=jnp.float32)
     hidden = (jax.nn.silu(gate_part) * lifted_part).astype(jnp.bfloat16)
     feed_terms = jnp.dot(
-        hidden,
-        lax.all_gather(down_weight, "sp", axis=1, tiled=True),
-        preferred_element_type=jnp.float32,
+        hidden, stack_and_merge(down_weight, "sp", 1), preferred_element_type=jnp.float32
     )
     feed = lax.psum_scatter(
         feed_terms.astype(jnp.bfloat16), "tp", scatter_dimension=1, tiled=True

time: 454 us -> 446 us (0.982)
  waiting for transfers between devices: 348 us -> 331 us
  local copies, waits for them, and re-layouts: 2.91 us -> 9.71 us
    all_gather x1, waiting for transfers between devices: 93.2 us -> 84.3 us  [stack_and_merge(): blocks = lax.all_gather(x, axis)]
    reshape x0 -> x1, local copies, waits for them, and re-layouts: none -> 8.33 us  [stack_and_merge(): return jnp.concatenate(blocks, axis=d)]
    all_gather x1, waiting for transfers between devices: 15.5 us -> 8.01 us  [body(): full_rows = lax.all_gather(normed_first, 'tp', axis=1, tiled=True)]
  transfers between devices with their start and end apart: 7 -> 7, of which waited for: 7 -> 7; matrix products, arithmetic and copies ran while one was open for 2% -> 5% of each run, Pallas kernels for 0% -> 0%
where the time goes in v1:
time: 446 us; the launch traced here: 445 us
  waiting for transfers between devices  331 us (74%)
  blocking collectives  44.4 us (10%)
  matrix products  34.4 us (8%)
  between operations  13.7 us (3%)
  other arithmetic  12 us (3%)
  local copies, waits for them, and re-layouts  9.71 us (2%)
    all_gather x1, waiting for transfers between devices, body(): lax.all_gather(gate_weight, 'sp', axis=0, tiled=True)  94.4 us
    all_gather x1, waiting for transfers between devices, body(): lax.all_gather(up_weight, 'sp', axis=0, tiled=True)  87.8 us
    all_gather x1, waiting for transfers between devices, stack_and_merge(): blocks = lax.all_gather(x, axis)  84.3 us
    all_gather x1, blocking collectives, body(): lax.all_gather(rotary_key, 'sp', axis=0, tiled=True)  32.8 us
    reduce_scatter x1, waiting for transfers between devices, body(): lax.psum_scatter(feed_terms.astype(jnp.bfloat16), 'tp', scatter_dimension...  23.2 us
    reduce_scatter x1, waiting for transfers between devices, body(): lax.psum_scatter(terms.astype(jnp.bfloat16), 'tp', scatter_dimension=1, t...  23 us
  transfers between devices with their start and end apart: 7, of which 7 were waited for; matrix products, arithmetic and copies ran while one was open for 5% of the time, Pallas kernels for 0%

profile of v1, /device:TPU:0, one launch (start us, length us, event | category | flops | bytes accessed | tf_op | source)
XLA Modules:
  0.0 445.1 jit_solution(17800248615906493966)
XLA Ops:
  6.5 0.7 all-gather.7.cloned.1.call-update
  7.3 0.0 reduce-scatter.3.cloned.1.call-start
  7.4 32.8 %all_gather.22 = bf16[2048,32]{0,1:T(8,128)(2,1)S(1)} all-gather(bf16[256,32]{0,1:T(8,128)(2,1)} %param.24), channel_id=1, replica_groups=mesh['sp'=8,'tp'=4] {'sp'}, dimensions={0}, use_global_device_ids=true | all-gather | bytes 147456 | tf_op jit(solution)/shard_map/all_gather | solution.py:132
  40.2 1.1 fusion.31
  41.3 1.3 convolution_bitcast_fusion.5
  42.6 1.3 convolution_bitcast_fusion.4
  43.9 0.2 fusion.97
  44.1 0.6 fusion.59
  44.7 0.5 convolution_bitcast_fusion.2
  45.2 7.4 %all-gather.7.cloned.1.call-done = bf16[2048,256]{1,0:T(8,128)(2,1)} async-done(((bf16[256,256]{1,0:T(8,128)(2,1)}), bf16[2048,256]{1,0:T(8,128)(2,1)}) %all-gather.7.cloned.1.call-update) | async-done | bytes 1048592 | tf_op jit(solution)/shard_map/all_gather | solution.py:131
  52.5 1.6 fusion.6
  54.2 3.4 fusion.132
  57.5 2.1 fusion.9
  59.7 2.2 convolution_bitcast_fusion.1
  61.9 2.1 fusion.131
  64.1 0.0 copy-start.14
  64.1 1.3 copy-done.2
  65.4 0.4 fusion.11
  65.8 2.6 fusion.22
  68.5 1.8 fusion.135
  70.2 2.5 fusion.24
  72.8 3.1 fusion.4
  75.9 0.0 reduce-scatter.3.cloned.1.call-update
  75.9 0.0 all-gather.15.cloned.1.call-start
  76.0 0.7 all-gather.15.cloned.1.call-update
  76.7 0.0 all-gather.9.cloned.1.call-start
  76.7 23.0 %reduce-scatter.3.cloned.1.call-done = bf16[256,512]{1,0:T(8,128)(2,1)} async-done(((bf16[256,2048]{1,0:T(8,128)(2,1)}), bf16[256,512]{1,0:T(8,128)(2,1)}) %reduce-scatter.3.cloned.1.call-update) | async-done | bytes 262160 | tf_op jit(solution)/shard_map/reduce_scatter | solution.py:170
  99.7 1.2 fusion.34
  100.9 5.8 %all-reduce.1 = (f32[256]{0:T(256)S(1)}, f32[256]{0:T(256)S(1)}) all-reduce(f32[256]{0:T(256)S(1)} %get-tuple-element.8, f32[256]{0:T(256)S(1)} %get-tuple-element.7), channel_id=1, replica_groups=mesh['sp'=8,'tp'=4] {'tp'}, use_global_device_ids=true, to_apply=%region_10.11 | all-reduce | flops 512 | bytes 4096 | tf_op jit(solution)/shard_map/psum | solution.py:175
  106.6 1.8 add_convert_fusion.1
  108.5 0.0 all-gather.9.cloned.1.call-update
  108.5 0.0 all-gather.11.cloned.1.call-start
  108.5 0.5 all-gather.11.cloned.1.call-update
  109.1 0.0 all-gather.13.cloned.1.call-start
  109.1 0.5 all-gather.13.cloned.1.call-update
  109.7 0.2 reduce-scatter.5.cloned.1.call-start
  109.9 84.3 %all-gather.15.cloned.1.call-done = bf16[11264,256]{1,0:T(8,128)(2,1)} async-done(((bf16[1408,256]{1,0:T(8,128)(2,1)}), bf16[11264,256]{1,0:T(8,128)(2,1)}) %all-gather.15.cloned.1.call-update) | async-done | bytes 5767184 | tf_op jit(solution)/shard_map/all_gather | solution.py:19
  194.2 8.3 %copy.28 = bf16[1408,8,256]{0,2,1:T(8,128)(2,1)} copy(bf16[1408,8,256]{2,0,1:T(8,128)(2,1)} %bitcast.104) | data formatting | bytes 11534336 | tf_op jit(solution)/shard_map/reshape | solution.py:20
  202.5 8.0 %all-gather.9.cloned.1.call-done = bf16[256,2048]{1,0:T(8,128)(2,1)} async-done(((bf16[256,512]{1,0:T(8,128)(2,1)}), bf16[256,2048]{1,0:T(8,128)(2,1)}) %all-gather.9.cloned.1.call-update) | async-done | bytes 1048592 | tf_op jit(solution)/shard_map/all_gather | solution.py:177
  210.6 94.4 %all-gather.11.cloned.1.call-done = bf16[2048,1408]{1,0:T(8,128)(2,1)} async-done(((bf16[256,1408]{1,0:T(8,128)(2,1)}), bf16[2048,1408]{1,0:T(8,128)(2,1)}) %all-gather.11.cloned.1.call-update) | async-done | bytes 5767184 | tf_op jit(solution)/shard_map/all_gather | solution.py:179
  304.9 4.8 %fusion.136 = f32[256,1408]{1,0:T(8,128)S(1)} fusion(bf16[256,2048]{1,0:T(8,128)(2,1)} %all-gather.9.cloned.1.call-done, bf16[2048,1408]{1,0:T(8,128)(2,1)} %all-gather.11.cloned.1.call-done), kind=kOutput, calls=%fused_computation.179 | convolution fusion | flops 1476395008 | bytes 8257536 | tf_op jit(solution)/shard_map/dot_general | solution.py:182
  309.7 87.8 %all-gather.13.cloned.1.call-done = bf16[2048,1408]{1,0:T(8,128)(2,1)} async-done(((bf16[256,1408]{1,0:T(8,128)(2,1)}), bf16[2048,1408]{1,0:T(8,128)(2,1)}) %all-gather.13.cloned.1.call-update) | async-done | bytes 5767184 | tf_op jit(solution)/shard_map/all_gather | solution.py:180
  397.5 8.8 %convolution_convert_fusion = bf16[256,2048]{1,0:T(8,128)(2,1)} fusion(bf16[1408,2048]{0,1:T(8,128)(2,1)} %bitcast.105, bf16[256,2048]{1,0:T(8,128)(2,1)S(1)} %copy-done.13, bf16[2048,1408]{1,0:T(8,128)(2,1)} %all-gather.13.cloned.1.call-done, f32[256,1408]{1,0:T(8,128)S(1)} %fusion.136), kind=kOutput, calls=%fused_computation.14 | convolution fusion | flops 2955476992 | bytes 15073280 | tf_op jit(solution)/shard_map/dot_general | solution.py:185
  406.3 0.0 reduce-scatter.5.cloned.1.call-update
  406.3 23.2 %reduce-scatter.5.cloned.1.call-done = bf16[256,512]{1,0:T(8,128)(2,1)} async-done(((bf16[256,2048]{1,0:T(8,128)(2,1)}), bf16[256,512]{1,0:T(8,128)(2,1)}) %reduce-scatter.5.cloned.1.call-update) | async-done | bytes 262160 | tf_op jit(solution)/shard_map/reduce_scatter | solution.py:188
  429.5 1.2 fusion.35
  430.6 5.8 %all-reduce = (f32[256]{0:T(256)S(1)}, f32[256]{0:T(256)S(1)}) all-reduce(f32[256]{0:T(256)S(1)} %get-tuple-element.6, f32[256]{0:T(256)S(1)} %get-tuple-element.5), channel_id=1, replica_groups=mesh['sp'=8,'tp'=4] {'tp'}, use_global_device_ids=true, to_apply=%region_15.16 | all-reduce | flops 512 | bytes 4096 | tf_op jit(solution)/shard_map/psum | solution.py:192
  436.4 1.8 add_convert_fusion
  (41 shorter events, 0.2 us)
Async XLA Ops:
  6.5 61.9 %copy-start = (bf16[128,2048]{1,0:T(8,128)(2,1)S(1)}, bf16[128,2048]{1,0:T(8,128)(2,1)}, u32[]{:S(2)}) copy-start(bf16[128,2048]{1,0:T(8,128)(2,1)} %param.34) | copy-start | bytes 1572868
  6.5 46.0 %all-gather.7.cloned.1.call-start = ((), (), s32[]{:S(2)}) async-start(), calls=%async_computation.2 | async-start | bytes 1179648 | tf_op jit(solution)/shard_map/all_gather | solution.py:131
  7.3 92.4 %reduce-scatter.3.cloned.1.call-start = ((), (), s32[]{:S(2)}) async-start(), calls=%async_computation.3 | async-start | bytes 1310720 | tf_op jit(solution)/shard_map/reduce_scatter | solution.py:170
  43.9 10.2 %copy-start.7 = (bf16[256,64]{0,1:T(8,128)(2,1)S(1)}, bf16[256,64]{0,1:T(8,128)(2,1)}, u32[]{:S(2)}) copy-start(bf16[256,64]{0,1:T(8,128)(2,1)} %param.28) | copy-start | bytes 98308
  43.9 10.2 %copy-start.8 = (f32[256]{0:T(256)S(1)}, f32[256]{0:T(256)}, u32[]{:S(2)}) copy-start(f32[256]{0:T(256)} %param.26) | copy-start | bytes 3076
  57.5 2.1 copy-start.1
  57.5 2.1 copy-start.6
  64.1 1.3 copy-start.2
  64.1 1.8 copy-start.14
  68.5 1.8 copy-start.15
  70.2 2.5 copy-start.5
  72.8 26.9 %copy-start.4 = (bf16[256,512]{1,0:T(8,128)(2,1)S(1)}, bf16[256,512]{1,0:T(8,128)(2,1)}, u32[]{:S(2)}) copy-start(bf16[256,512]{1,0:T(8,128)(2,1)} %param.21) | copy-start | bytes 786436
  72.8 33.8 %copy-start.9 = (f32[512]{0:T(512)S(1)}, f32[512]{0:T(512)}, u32[]{:S(2)}) copy-start(f32[512]{0:T(512)} %param.36) | copy-start | bytes 6148
  72.8 33.8 %copy-start.10 = (f32[512]{0:T(512)S(1)}, f32[512]{0:T(512)}, u32[]{:S(2)}) copy-start(f32[512]{0:T(512)} %param.35) | copy-start | bytes 6148
  75.9 118.3 %all-gather.15.cloned.1.call-start = ((), (), s32[]{:S(2)}) async-start(), calls=%async_computation.8 | async-start | bytes 6488064 | tf_op jit(solution)/shard_map/all_gather | solution.py:19
  76.7 133.9 %all-gather.9.cloned.1.call-start = ((), (), s32[]{:S(2)}) async-start(), calls=%async_computation.4 | async-start | bytes 1310720 | tf_op jit(solution)/shard_map/all_gather | solution.py:177
  108.5 196.4 %all-gather.11.cloned.1.call-start = ((), (), s32[]{:S(2)}) async-start(), calls=%async_computation.5 | async-start | bytes 6488064 | tf_op jit(solution)/shard_map/all_gather | solution.py:179
  109.1 288.4 %all-gather.13.cloned.1.call-start = ((), (), s32[]{:S(2)}) async-start(), calls=%async_computation.6 | async-start | bytes 6488064 | tf_op jit(solution)/shard_map/all_gather | solution.py:180
  109.7 319.8 %reduce-scatter.5.cloned.1.call-start = ((), (), s32[]{:S(2)}) async-start(), calls=%async_computation.7 | async-start | bytes 1310720 | tf_op jit(solution)/shard_map/reduce_scatter | solution.py:188
  210.6 186.9 %copy-start.13 = (bf16[256,2048]{1,0:T(8,128)(2,1)S(1)}, bf16[256,2048]{1,0:T(8,128)(2,1)}, u32[]{:S(2)}) copy-start(bf16[256,2048]{1,0:T(8,128)(2,1)} %all-gather.9.cloned.1.call-done) | copy-start | bytes 3145732
  397.5 32.0 %copy-start.3 = (bf16[256,512]{1,0:T(8,128)(2,1)S(1)}, bf16[256,512]{1,0:T(8,128)(2,1)}, u32[]{:S(2)}) copy-start(bf16[256,512]{1,0:T(8,128)(2,1)} %add_convert_fusion.1) | copy-start | bytes 786436
  397.5 38.9 %copy-start.11 = (f32[512]{0:T(512)S(1)}, f32[512]{0:T(512)}, u32[]{:S(2)}) copy-start(f32[512]{0:T(512)} %param.41) | copy-start | bytes 6148
  397.5 38.9 %copy-start.12 = (f32[512]{0:T(512)S(1)}, f32[512]{0:T(512)}, u32[]{:S(2)}) copy-start(f32[512]{0:T(512)} %param.40) | copy-start | bytes 6148
Sparse Core Ops, SparseCore 0:
  9.5 43.0 all-gather.6
  76.1 23.6 reduce-scatter.2
  101.9 92.2 all-gather.14
  195.6 14.8 all-gather.8
  212.6 92.2 all-gather.10
  307.0 90.4 all-gather.12
  406.4 22.9 reduce-scatter.4
